TPU v7x, 32 devices: a whole 2x2x4 slice. The times are simulated.
32 devices in a mesh: kv: 8 (over z, x), tp: 4 (over y, core).
Axes of the slice: x: 2, y: 2, z: 4, core: 2. Of those that a mesh axis runs over, the one named last changes fastest.
Arguments:
- tokens: bfloat16 [22, 4096], P(None, ('kv', 'tp')), may hold values from -22 to 22
- attn_gain: float32 [4096], P('kv'), may hold values from 0.1 to 1.9
- w_query: bfloat16 [4096, 4096], P('kv', 'tp'), may hold values from -0.09375 to 0.09375
- w_key: bfloat16 [4096, 4096], P('kv', 'tp'), may hold values from -0.5 to 0.5
- w_value: bfloat16 [4096, 4096], P('kv', 'tp'), may hold values from -0.09375 to 0.09375
- cache_keys: bfloat16 [22, 2048, 32, 128], P(None, 'kv', 'tp'), may hold values from -256 to 256
- cache_values: bfloat16 [22, 2048, 32, 128], P(None, 'kv', 'tp'), may hold values from -6 to 6
- lambdas: float32 [32], P('tp'), may hold values from 0.3 to 0.8
- head_gain: float32 [128], replicated, may hold values from 0.1 to 1.9
- w_out: bfloat16 [4096, 4096], P('tp', 'kv'), may hold values from -0.09375 to 0.09375
- mlp_gain: float32 [4096], P('kv'), may hold values from 0.1 to 1.9
- w_gate: bfloat16 [4096, 11008], P('kv', 'tp'), may hold values from -0.09375 to 0.09375
- w_up: bfloat16 [4096, 11008], P('kv', 'tp'), may hold values from -0.09375 to 0.09375
- w_down: bfloat16 [11008, 4096], P('tp', 'kv'), may hold values from -0.0546875 to 0.0546875
Outputs:
- output: bfloat16 [22, 4096], P(None, ('kv', 'tp'))
All inputs are finite; a program needn't handle non-finite values.
Results may differ from a plain program's by a relative error of at most 0.017.
The roundings to bfloat16 on the way count: a program that leaves them out, or rounds other values in their place, can miss the bound.
Values may be sent and summed in bfloat16 or wider, within the bound.
A program may use at most 128 MiB of HBM per device.

v0:
```python
import jax
import jax.numpy as jnp
from jax import lax
from jax.sharding import PartitionSpec as P

D = 4096


epsilon = 1e-06


def combined_all(value, axis, join):
    pieces = jax.tree.map(lambda part: lax.all_gather(part, axis), value)
    head = jax.tree.map(lambda part: part[0], pieces)
    tail = jax.tree.map(lambda part: part[1:], pieces)
    running, _ = lax.scan(lambda running, section: (join(running, section), None), head, tail)
    return running


def join_map(left_max, left_sum, left_val, right_max, right_sum, right_val):
    peak_val = jnp.maximum(left_max, right_max)
    left_weight = jnp.exp(left_max - peak_val)
    right_weight = jnp.exp(right_max - peak_val)
    return (
        peak_val,
        left_sum * left_weight + right_sum * right_weight,
        left_val * left_weight[..., None] + right_val * right_weight[..., None],
    )


def combine(earlier, later):
    return join_map(earlier[0], earlier[1], earlier[2], later[0], later[1], later[2]) + join_map(
        earlier[3], earlier[4], earlier[5], later[3], later[4], later[5]
    )


def per_device(
    tokens,
    attn_gain,
    w_query,
    w_key,
    w_value,
    cache_keys,
    cache_values,
    lambdas,
    head_gain,
    w_out,
    mlp_gain,
    w_gate,
    w_up,
    w_down,
):
    seq_count = tokens.shape[0]
    own_width = tokens.shape[1]
    local_heads = lambdas.shape[0]
    head_dim = head_gain.shape[0]
    half_dim = head_dim // 2
    score_scale = half_dim ** (-0.5)
    gathered = lax.all_gather(tokens, "tp", axis=1, tiled=True)
    gathered_f = gathered.astype(jnp.float32)
    normed_in = (gathered_f * attn_gain).astype(jnp.bfloat16)
    query_part = jnp.dot(normed_in, w_query, preferred_element_type=jnp.float32)
    key_part = jnp.dot(normed_in, w_key, preferred_element_type=jnp.float32)
    value_part = jnp.dot(normed_in, w_value, preferred_element_type=jnp.float32)
    query_sum, key_sum, value_sum, square_sum = lax.psum(
        (query_part, key_part, value_part, jnp.sum(gathered_f * gathered_f, axis=1, keepdims=True)),
        "kv",
    )
    scale_in = lax.rsqrt(square_sum / D + epsilon)
    query_rows = (
        (scale_in * query_sum).astype(jnp.bfloat16).reshape(seq_count, local_heads, head_dim)
    )
    key_new = (scale_in * key_sum).astype(jnp.bfloat16).reshape(seq_count, local_heads, head_dim)
    value_new = (
        (scale_in * value_sum).astype(jnp.bfloat16).reshape(seq_count, local_heads, head_dim)
    )

    def partial_map(low, high):
        scores = (
            jnp.einsum(
                "shd,sthd->sht",
                query_rows[:, :, low:high],
                cache_keys[:, :, :, low:high],
                preferred_element_type=jnp.float32,
            )
            * score_scale
        )
        maxima = jnp.max(scores, axis=2)
        weights = jnp.exp(scores - maxima[:, :, None])
        totals = jnp.sum(weights, axis=2)
        summed = jnp.einsum(
            "sht,sthd->shd",
            weights.astype(jnp.bfloat16),
            cache_values,
            preferred_element_type=jnp.float32,
        )
        return (maxima, totals, summed)

    def own_term(low, high):
        score_new = (
            jnp.sum(
                query_rows[:, :, low:high].astype(jnp.float32)
                * key_new[:, :, low:high].astype(jnp.float32),
                axis=2,
            )
            * score_scale
        )
        return (score_new, jnp.ones_like(score_new), value_new.astype(jnp.float32))

    first_part = partial_map(0, half_dim)
    second_part = partial_map(half_dim, head_dim)
    merged = combined_all(
        (
            first_part[0],
            first_part[1],
            first_part[2],
            second_part[0],
            second_part[1],
            second_part[2],
        ),
        "kv",
        combine,
    )
    combined = combine(merged, own_term(0, half_dim) + own_term(half_dim, head_dim))
    first_map = combined[2] / combined[1][:, :, None]
    second_map = combined[5] / combined[4][:, :, None]
    difference = first_map - lambdas[None, :, None] * second_map
    normed = (
        difference
        * lax.rsqrt(jnp.mean(difference * difference, axis=2, keepdims=True) + epsilon)
        * head_gain
    )
    heads_out = normed.astype(jnp.bfloat16).reshape(seq_count, local_heads * head_dim)
    branch = lax.psum(
        jnp.dot(heads_out, w_out, preferred_element_type=jnp.float32).astype(jnp.bfloat16), "tp"
    ).astype(jnp.float32)
    residual = (gathered_f + branch).astype(jnp.bfloat16)
    residual_f = residual.astype(jnp.float32)
    mid_sum = lax.psum(jnp.sum(residual_f * residual_f, axis=1, keepdims=True), "kv")
    scale_mid = lax.rsqrt(mid_sum / D + epsilon)
    normed_mid = (residual_f * mlp_gain).astype(jnp.bfloat16)
    gate_part = jnp.dot(normed_mid, w_gate, preferred_element_type=jnp.float32)
    up_part = jnp.dot(normed_mid, w_up, preferred_element_type=jnp.float32)
    gate_sum, up_sum = lax.psum((gate_part, up_part), "kv")
    hidden = (jax.nn.silu(scale_mid * gate_sum) * (scale_mid * up_sum)).astype(jnp.bfloat16)
    down_part = jnp.dot(hidden, w_down, preferred_element_type=jnp.float32).astype(jnp.bfloat16)
    mixer_own = lax.psum_scatter(down_part, "tp", scatter_dimension=1, tiled=True).astype(
        jnp.float32
    )
    tp_index = lax.axis_index("tp")
    residual_own = lax.dynamic_slice_in_dim(residual_f, tp_index * own_width, own_width, 1)
    return (residual_own + mixer_own).astype(jnp.bfloat16)


def solution(mesh):
    in_specs = (
        P(None, ("kv", "tp")),
        P("kv"),
        P("kv", "tp"),
        P("kv", "tp"),
        P("kv", "tp"),
        P(None, "kv", "tp", None),
        P(None, "kv", "tp", None),
        P("tp"),
        P(),
        P("tp", "kv"),
        P("kv"),
        P("kv", "tp"),
        P("kv", "tp"),
        P("tp", "kv"),
    )
    out_specs = P(None, ("kv", "tp"))
    return jax.shard_map(
        per_device, mesh=mesh, in_specs=in_specs, out_specs=out_specs, check_vma=False
    )
```

profile of v0, /device:TPU:0, one launch (start us, length us, event | category | flops | bytes accessed | tf_op | source)
XLA Modules:
  0.0 441.2 jit_solution(7946327300778123110)
XLA Ops:
  6.5 6.5 %all_gather.39 = bf16[22,512]{1,0:T(8,128)(2,1)S(1)} all-gather(bf16[22,128]{1,0:T(8,128)(2,1)} %param.16), channel_id=1, replica_groups=mesh['kv'=8,'tp'=4] {'tp'}, dimensions={1}, use_global_device_ids=true | all-gather | bytes 28160 | tf_op jit(solution)/shard_map/all_gather | solution.py:59
  13.0 2.1 fusion.35
  15.2 2.1 fusion.33
  17.3 2.1 fusion.37
  19.5 17.3 %fusion.54 = (bf16[22,256,8,64]{3,2,1,0:T(8,128)(2,1)}, bf16[22,256,8,64]{3,2,1,0:T(8,128)(2,1)}) fusion(bf16[22,256,8,128]{3,2,1,0:T(8,128)(2,1)} %param.21), kind=kLoop, calls=%fused_computation.89 | loop fusion | bytes 23068672 | tf_op jit(solution)/shard_map/slice | solution.py:83
  36.8 0.1 fusion.28
  36.9 22.2 %psum.56 = f32[22,1]{0,1:T(1,128)S(1)} all-reduce(f32[22,1]{0,1:T(1,128)S(1)} %bitcast.129), channel_id=1, replica_groups=mesh['kv'=8,'tp'=4] {'kv'}, use_global_device_ids=true, to_apply=%region_1.0 | all-reduce | flops 22 | bytes 176 | tf_op jit(solution)/shard_map/psum | solution.py:65
  59.1 34.2 %all-reduce.7.cloned.1.call-done = (f32[22,1024]{1,0:T(8,128)}, f32[22,1024]{1,0:T(8,128)}, f32[22,1024]{1,0:T(8,128)}) async-done(((f32[22,1024]{1,0:T(8,128)}, f32[22,1024]{1,0:T(8,128)}, f32[22,1024]{1,0:T(8,128)}), (f32[22,1024]{1,0:T(8,128)}, f32[22,1024]{1,0:T(8,128)}, f32[22,1024]{1,0:T(8,128)})) %all-reduce.7.cloned.1.call-update) | async-done | bytes 270352 | tf_op jit(solution)/shard_map/psum | solution.py:65
  93.3 1.1 fusion.31
  94.5 7.4 %fusion.6 = f32[22,8,1,256]{3,2,1,0:T(1,128)S(1)} fusion(bf16[22,256,8,64]{3,2,1,0:T(8,128)(2,1)} %get-tuple-element.134, bf16[22,8,64,1]{2,1,0,3:T(8,128)(2,1)S(1)} %get-tuple-element.142), kind=kOutput, calls=%fused_computation.16 | convolution fusion | flops 5767168 | bytes 5969920 | tf_op jit(solution)/shard_map/shd,sthd->sht/dot_general | solution.py:80
  101.8 0.1 fusion.21
  101.9 0.2 fusion.24
  102.2 30.6 %all-gather.8 = f32[8,22,8]{1,2,0:T(8,128)S(1)} all-gather(f32[1,22,8]{1,2,0:T(8,128)S(1)} %copy.59), channel_id=5, replica_groups=mesh['kv'=8,'tp'=4] {'kv'}, dimensions={0}, use_global_device_ids=true | all-gather | bytes 6336 | tf_op jit(solution)/shard_map/all_gather | solution.py:13
  132.9 30.6 %all-gather.9 = f32[8,22,8]{1,2,0:T(8,128)S(1)} all-gather(f32[1,22,8]{1,2,0:T(8,128)S(1)} %copy.60), channel_id=6, replica_groups=mesh['kv'=8,'tp'=4] {'kv'}, dimensions={0}, use_global_device_ids=true | all-gather | bytes 6336 | tf_op jit(solution)/shard_map/all_gather | solution.py:13
  163.5 7.4 %fusion.8 = f32[22,8,1,256]{3,2,1,0:T(1,128)S(1)} fusion(bf16[22,256,8,64]{3,2,1,0:T(8,128)(2,1)} %get-tuple-element.135, bf16[22,8,64,1]{2,1,0,3:T(8,128)(2,1)S(1)} %get-tuple-element.143), kind=kOutput, calls=%fused_computation.18 | convolution fusion | flops 5767168 | bytes 5969920 | tf_op jit(solution)/shard_map/shd,sthd->sht/dot_general | solution.py:80
  170.8 0.1 fusion.20
  171.0 0.2 fusion.25
  171.2 30.6 %all-gather.6 = f32[8,22,8]{1,2,0:T(8,128)S(1)} all-gather(f32[1,22,8]{1,2,0:T(8,128)S(1)} %copy.57), channel_id=2, replica_groups=mesh['kv'=8,'tp'=4] {'kv'}, dimensions={0}, use_global_device_ids=true | all-gather | bytes 6336 | tf_op jit(solution)/shard_map/all_gather | solution.py:13
  201.9 30.6 %all-gather.7 = f32[8,22,8]{1,2,0:T(8,128)S(1)} all-gather(f32[1,22,8]{1,2,0:T(8,128)S(1)} %copy.58), channel_id=3, replica_groups=mesh['kv'=8,'tp'=4] {'kv'}, dimensions={0}, use_global_device_ids=true | all-gather | bytes 6336 | tf_op jit(solution)/shard_map/all_gather | solution.py:13
  232.5 5.9 %fusion.12 = f32[22,8,1,128]{3,2,1,0:T(1,128)S(1)} fusion(bf16[22,256,8,128]{3,2,1,0:T(8,128)(2,1)} %param.22, bf16[22,8,256,1]{2,1,0,3:T(8,128)(2,1)S(1)} %get-tuple-element.138), kind=kOutput, calls=%fused_computation.22 | convolution fusion | flops 11534336 | bytes 11714560 | tf_op jit(solution)/shard_map/sht,sthd->shd/dot_general | solution.py:91
  238.5 32.1 %all-gather.2 = f32[176,8,128]{2,1,0:T(8,128)S(1)} all-gather(f32[22,8,128]{2,1,0:T(8,128)S(1)} %bitcast.123), channel_id=4, replica_groups=mesh['kv'=8,'tp'=4] {'kv'}, dimensions={0}, use_global_device_ids=true | all-gather | bytes 811008 | tf_op jit(solution)/shard_map/all_gather | solution.py:13
  270.5 0.9 slice.104
  271.4 5.9 %fusion.10 = f32[22,8,1,128]{3,2,1,0:T(1,128)S(1)} fusion(bf16[22,256,8,128]{3,2,1,0:T(8,128)(2,1)} %param.22, bf16[22,8,256,1]{2,1,0,3:T(8,128)(2,1)S(1)} %get-tuple-element.136), kind=kOutput, calls=%fused_computation.20 | convolution fusion | flops 11534336 | bytes 11714560 | tf_op jit(solution)/shard_map/sht,sthd->shd/dot_general | solution.py:91
  277.3 31.7 %all-gather.5 = f32[176,8,128]{2,1,0:T(8,128)S(1)} all-gather(f32[22,8,128]{2,1,0:T(8,128)S(1)} %bitcast.124), channel_id=7, replica_groups=mesh['kv'=8,'tp'=4] {'kv'}, dimensions={0}, use_global_device_ids=true | all-gather | bytes 811008 | tf_op jit(solution)/shard_map/all_gather | solution.py:13
  309.0 0.9 slice.107
  309.9 0.2 multiply_reduce_fusion.2
  310.2 10.7 %while.20 = (s32[]{:T(128)}, f32[22,8]{0,1:T(8,128)S(1)}, f32[22,8]{0,1:T(8,128)S(1)}, f32[22,8,128]{2,1,0:T(8,128)S(1)}, f32[22,8]{0,1:T(8,128)S(1)}, /*index=5...) while((s32[]{:T(128)}, f32[22,8]{0,1:T(8,128)S(1)}, ...), condition=%wide.region_8.0_spmd, body=%wide.region_7.0_spmd.sunk | while | flops 137282 | bytes 560537 | solution.py:16
  310.6 1.1 fusion.68
  312.1 1.1 fusion.68
  313.7 1.1 fusion.68
  315.2 1.1 fusion.68
  316.7 1.1 fusion.68
  318.3 1.1 fusion.68
  319.8 1.1 fusion.68
  321.5 0.3 multiply_reduce_fusion
  321.8 0.1 multiply_convert_fusion.5
  321.9 1.5 convolution_convert_fusion.1
  323.4 10.3 %psum.60 = bf16[22,512]{1,0:T(8,128)(2,1)S(1)} all-reduce(bf16[22,512]{1,0:T(8,128)(2,1)S(1)} %convolution_convert_fusion.1), channel_id=1, replica_groups=mesh['kv'=8,'tp'=4] {'tp'}, use_global_device_ids=true, to_apply=%region_14.15 | all-reduce | flops 11264 | bytes 45056 | tf_op jit(solution)/shard_map/psum | solution.py:134
  333.7 1.6 fusion.40
  335.2 3.4 fusion.39
  338.7 0.1 fusion.32
  338.8 19.8 %psum.61 = f32[22,1]{0,1:T(1,128)S(1)} all-reduce(f32[22,1]{0,1:T(1,128)S(1)} %bitcast.128), channel_id=1, replica_groups=mesh['kv'=8,'tp'=4] {'kv'}, use_global_device_ids=true, to_apply=%region_16.17 | all-reduce | flops 22 | bytes 176 | tf_op jit(solution)/shard_map/psum | solution.py:139
  358.6 52.5 %all-reduce.5.cloned.1.call-done = (f32[22,2752]{1,0:T(8,128)}, f32[22,2752]{1,0:T(8,128)}) async-done(((f32[22,2752]{1,0:T(8,128)}, f32[22,2752]{1,0:T(8,128)}), (f32[22,2752]{1,0:T(8,128)}, f32[22,2752]{1,0:T(8,128)})) %all-reduce.5.cloned.1.call-update) | async-done | bytes 484368 | tf_op jit(solution)/shard_map/psum | solution.py:144
  411.1 2.5 convolution_convert_fusion
  413.6 0.8 copy.80
  414.4 18.8 %reduce-scatter.4.cloned.1.call-done = bf16[128,22]{1,0:T(8,128)(2,1)} async-done(((bf16[512,22]{1,0:T(8,128)(2,1)}), bf16[128,22]{1,0:T(8,128)(2,1)}) %reduce-scatter.4.cloned.1.call-update) | async-done | bytes 5648
  433.2 0.8 copy.81
  434.0 0.6 add_convert_fusion
  (96 shorter events, 3.9 us)
Async XLA Ops:
  6.5 327.1 %copy-start = (bf16[512,2752]{0,1:T(8,128)(2,1)S(1)}, bf16[512,2752]{0,1:T(8,128)(2,1)}, u32[]{:S(2)}) copy-start(bf16[512,2752]{0,1:T(8,128)(2,1)} %param.27) | copy-start | bytes 8454148
  6.5 86.7 %all-reduce.7.cloned.1.call-start = ((), (), s32[]{:S(2)}) async-start(), calls=%async_computation.3 | async-start | bytes 589824 | tf_op jit(solution)/shard_map/psum | solution.py:65
  19.5 391.6 %all-reduce.5.cloned.1.call-start = ((), (), s32[]{:S(2)}) async-start(), calls=%async_computation.2 | async-start | bytes 1081344 | tf_op jit(solution)/shard_map/psum | solution.py:144
  132.8 105.6 %copy-start.1 = (f32[8,22,8]{1,2,0:T(8,128)}, f32[8,22,8]{1,2,0:T(8,128)S(1)}, u32[]{:S(2)}) copy-start(f32[8,22,8]{1,2,0:T(8,128)S(1)} %all-gather.8) | copy-start | bytes 16900
  163.5 74.9 %copy-start.2 = (f32[8,22,8]{1,2,0:T(8,128)}, f32[8,22,8]{1,2,0:T(8,128)S(1)}, u32[]{:S(2)}) copy-start(f32[8,22,8]{1,2,0:T(8,128)S(1)} %all-gather.9) | copy-start | bytes 16900
  238.4 83.1 %copy-start.5 = (f32[8]{0:T(128)S(1)}, f32[8]{0:T(128)}, u32[]{:S(2)}) copy-start(f32[8]{0:T(128)} %param.23) | copy-start | bytes 100
  238.4 83.4 %copy-start.4 = (f32[128]{0:T(128)S(1)}, f32[128]{0:T(128)}, u32[]{:S(2)}) copy-start(f32[128]{0:T(128)} %param.24) | copy-start | bytes 1540
  238.4 71.8 %slice-start = ((f32[8,22,8]{1,2,0:T(8,128)}), f32[7,22,8]{1,2,0:T(8,128)S(1)}, s32[]{:S(2)}) async-start(f32[8,22,8]{1,2,0:T(8,128)} %copy-done.1), calls=%async_computation.4 | async-start | bytes 57344 | tf_op jit(solution)/shard_map/slice | solution.py:15
  238.4 71.8 %slice-start.1 = ((f32[8,22,8]{1,2,0:T(8,128)}), f32[7,22,8]{1,2,0:T(8,128)S(1)}, s32[]{:S(2)}) async-start(f32[8,22,8]{1,2,0:T(8,128)} %copy-done.2), calls=%async_computation.5 | async-start | bytes 57344 | tf_op jit(solution)/shard_map/slice | solution.py:15
  238.4 95.2 %copy-start.3 = (f32[512]{0:T(512)S(1)}, f32[512]{0:T(512)}, u32[]{:S(2)}) copy-start(f32[512]{0:T(512)} %param.26) | copy-start | bytes 6148
  338.6 94.6 %reduce-scatter.4.cloned.1.call-start = ((), (), s32[]{:S(2)}) async-start(), calls=%async_computation.1 | async-start | bytes 163840
Sparse Core Ops, SparseCore 0:
  19.6 73.6 all-reduce.6
  338.7 72.3 all-reduce.4
  414.5 18.6 reduce-scatter.3
where the time goes:
time: 442 us; the launch traced here: 441 us
  blocking collectives  245 us (55%)
  waiting for transfers between devices  105 us (24%)
  matrix products  41.8 us (9%)
  local copies, waits for them, and re-layouts  24.2 us (5%)
  between operations  13.3 us (3%)
  other arithmetic  11.2 us (3%)
    all_gather x6, blocking collectives, combined_all(): pieces = jax.tree.map(lambda part: lax.all_gather(part, axis), value)  186 us
    psum x1, waiting for transfers between devices, per_device(): gate_sum, up_sum = lax.psum((gate_part, up_part), 'kv')  52.5 us
    psum x1, waiting for transfers between devices, per_device(): lax.psum((query_part, key_part, value_part, jnp.sum(gathered_f * gathered...  34.2 us
    psum x1, blocking collectives, per_device(): lax.psum((query_part, key_part, value_part, jnp.sum(gathered_f * gathered...  22.2 us
    psum x1, blocking collectives, per_device(): lax.psum(jnp.sum(residual_f * residual_f, axis=1, keepdims=True), 'kv')  19.8 us
    unnamed x4, waiting for transfers between devices  18.8 us
    slice x1, local copies, waits for them, and re-layouts, partial_map(): cache_keys[:, :, :, low:high]  17.3 us
    dot_general x2, matrix products, partial_map(): jnp.einsum('shd,sthd->sht', query_rows[:, :, low:high], cache_keys[:, :,...  14.7 us
  transfers between devices with their start and end apart: 3, of which 3 were waited for; matrix products, arithmetic and copies ran while one was open for 4% of the time, Pallas kernels for 0%

commit v1 on v0

v1 whole, which is shorter than its diff:
```python
import functools

import jax
import jax.numpy as jnp
from jax import lax
from jax.experimental import pallas as pl
from jax.experimental.pallas import tpu as pltpu
from jax.sharding import PartitionSpec as P

epsilon = 1e-06
MESH = pl.DeviceIdType.MESH
F32 = jnp.float32
BF16 = jnp.bfloat16
QKV_LINK = jnp.float32
FF_LINK = jnp.bfloat16


def peers(axis, count):
    me = lax.axis_index(axis)
    return [(step, lax.rem(me + step, count)) for step in range(1, count)]


def greet(n_kv, n_tp):
    barrier = pltpu.get_barrier_semaphore()
    for axis, count in (("kv", n_kv), ("tp", n_tp)):
        for _, peer in peers(axis, count):
            pl.semaphore_signal(barrier, inc=1, device_id={axis: peer}, device_id_type=MESH)
    pl.semaphore_wait(barrier, n_kv + n_tp - 2)


def exchange(axis, count, source, target, send_sem, recv_sem):
    copies = []
    for step, peer in peers(axis, count):
        copy = pltpu.make_async_remote_copy(
            src_ref=source(peer),
            dst_ref=target,
            send_sem=send_sem.at[step - 1],
            recv_sem=recv_sem.at[step - 1],
            device_id={axis: peer},
            device_id_type=MESH,
        )
        copy.start()
        copies.append(copy)
    return copies


def wait_recv(copies):
    for copy in copies:
        copy.wait_recv()


def wait_send(copies):
    for copy in copies:
        copy.wait_send()


def pad_rows(value, rows):
    if value.shape[0] == rows:
        return value
    return jnp.concatenate(
        [value, jnp.zeros((rows - value.shape[0],) + value.shape[1:], value.dtype)], axis=0
    )


def pad_cols(value, cols):
    if value.shape[1] == cols:
        return value
    return jnp.concatenate(
        [value, jnp.zeros((value.shape[0], cols - value.shape[1]), value.dtype)], axis=1
    )


def project_kernel(
    dims, tok, gain, wq, wk, wv, x_out, q_out, k_out, v_out,
    wbuf, tok_all, sq_all, part, got, w_sem, t_s, t_r, s_s, s_r, p_s, p_r, q_s, q_r,
):
    n_kv, n_tp, groups, rows, width = dims
    seqs = tok.shape[0]
    hd = q_out.shape[2]
    loads = []
    for index, ref in enumerate((wq, wk, wv)):
        load = pltpu.make_async_copy(ref, wbuf.at[index], w_sem.at[index])
        load.start()
        loads.append(load)
    greet(n_kv, n_tp)
    me = lax.axis_index("kv")
    me_tp = lax.axis_index("tp")
    tok_copies = exchange("tp", n_tp, lambda peer: tok, tok_all.at[me_tp], t_s, t_r)
    tok_all[me_tp] = tok[...]
    wait_recv(tok_copies)
    x = jnp.concatenate([tok_all[index] for index in range(n_tp)], axis=1)
    x_out[...] = x
    xf = x.astype(F32)
    sq_all[me] = jnp.broadcast_to(jnp.sum(xf * xf, axis=1, keepdims=True), (seqs, 128))
    sq_copies = exchange("kv", n_kv, lambda peer: sq_all.at[me], sq_all.at[me], s_s, s_r)
    normed = (xf * gain[...]).astype(BF16)
    for index in range(3):
        loads[index].wait()
        product = jnp.dot(normed, wbuf[index], preferred_element_type=F32).astype(QKV_LINK)
        product = pad_rows(product, groups * rows)
        for owner in range(n_kv):
            head, group = owner // groups, owner % groups
            part[owner, index] = product[
                group * rows : (group + 1) * rows, head * hd : (head + 1) * hd
            ]
    part_copies = exchange("kv", n_kv, lambda peer: part.at[peer], got.at[me], p_s, p_r)
    got[me] = part[me]
    wait_recv(sq_copies)
    square = sq_all[0]
    for index in range(1, n_kv):
        square = square + sq_all[index]
    scale = lax.rsqrt(square[:, :1] / width + epsilon)
    if groups > 1:
        scale = pad_rows(scale, groups * rows)
        group_of = lax.rem(me, groups)
        mine = scale[:rows]
        for group in range(1, groups):
            mine = jnp.where(group_of == group, scale[group * rows : (group + 1) * rows], mine)
        scale = mine
    wait_recv(part_copies)
    for index in range(3):
        total = got[0, index].astype(F32)
        for owner in range(1, n_kv):
            total = total + got[owner, index].astype(F32)
        value = (scale * total).astype(BF16)
        if index == 0:
            q_out[me] = value
            q_copies = exchange("kv", n_kv, lambda peer: q_out.at[me], q_out.at[me], q_s, q_r)
        elif index == 1:
            k_out[...] = value
        else:
            v_out[...] = value
    wait_recv(q_copies)
    wait_send(tok_copies + sq_copies + part_copies + q_copies)


def attend_kernel(heads, per_step, q, keys, values, o_out, l_out, acc, lse):
    step = pl.program_id(0)
    length = keys.shape[1]
    hd = keys.shape[2]
    scale = (hd // 2) ** (-0.5)
    row = lax.broadcasted_iota(jnp.int32, (2 * heads, length), 0)
    col = lax.broadcasted_iota(jnp.int32, (2 * heads, length), 1)
    keep = lax.rem(col, heads) == lax.rem(row, heads)
    lane = lax.broadcasted_iota(jnp.int32, (2 * heads, 128), 1)

    @pl.when(step == 0)
    def _():
        lse[...] = jnp.zeros_like(lse)

    for index in range(per_step):
        seq = step * per_step + index
        scores = lax.dot_general(
            q[index], keys[index], (((1,), (1,)), ((), ())), preferred_element_type=F32
        )
        scores = jnp.where(keep, scores * scale, -1e30)
        peak = jnp.max(scores, axis=1, keepdims=True)
        weights = jnp.where(keep, jnp.exp(scores - peak), 0.0)
        total = jnp.sum(weights, axis=1, keepdims=True)
        summed = jnp.dot(weights.astype(BF16), values[index], preferred_element_type=F32)
        result = summed / total
        acc[:, pl.ds(seq, 1), :] = result[:, None, :]
        lse[...] = jnp.where(lane == seq, peak + jnp.log(total), lse[...])

    @pl.when(step == pl.num_programs(0) - 1)
    def _():
        stats = lse[...]
        l_out[...] = jnp.zeros_like(l_out)
        for head in range(heads):
            for half in range(2):
                at = half * heads + head
                o_out[head, half] = acc[at].astype(BF16)
                l_out[head, half : half + 1, :] = stats[at : at + 1, :]


def finish_kernel(
    dims, lam, o_in, l_in, q_all, k_own, v_own, head_gain, x, mid_gain, w_out, w_gate, w_up, w_down,
    out,
    wo, wg, wu, wd, o_all, l_all, h_all, b_all, sq_all, gu_part, gu_all, hid_all, d_part, d_all,
    w_sem, o_s, o_r, l_s, l_r, h_s, h_r, b_s, b_r, s_s, s_r, g_s, g_r, i_s, i_r, d_s, d_r,
):
    n_kv, n_tp, groups, rows, width, chunk = dims
    seqs = x.shape[0]
    hd = k_own.shape[1]
    loads = []
    for index, (ref, buf) in enumerate(((w_out, wo), (w_gate, wg), (w_up, wu), (w_down, wd))):
        load = pltpu.make_async_copy(ref, buf, w_sem.at[index])
        load.start()
        loads.append(load)
    greet(n_kv, n_tp)
    me = lax.axis_index("kv")
    me_tp = lax.axis_index("tp")
    l_copies = exchange("kv", n_kv, lambda peer: l_in.at[peer], l_all.at[me], l_s, l_r)
    o_copies = exchange("kv", n_kv, lambda peer: o_in.at[peer], o_all.at[me], o_s, o_r)
    l_all[me] = l_in[me]
    o_all[me] = o_in[me]
    product = q_all[me].astype(F32) * k_own[...].astype(F32)
    lane = lax.broadcasted_iota(jnp.int32, product.shape, 1)
    low = jnp.where(lane < hd // 2, product, 0.0)
    high = jnp.where(lane < hd // 2, 0.0, product)
    fresh = [
        jnp.sum(half, axis=1, keepdims=True) * ((hd // 2) ** (-0.5)) for half in (low, high)
    ]
    value_new = v_own[...].astype(F32)
    wait_recv(l_copies)
    stats = []
    for start in range(0, n_kv, 16):
        owners = range(start, min(start + 16, n_kv))
        stacked = pad_rows(jnp.concatenate([l_all[owner] for owner in owners], axis=0), 128)
        turned = jnp.transpose(stacked)
        stats += [turned[:rows, 8 * at : 8 * at + 2] for at in range(len(owners))]
    wait_recv(o_copies)
    maps = []
    for half in range(2):
        levels = [stat[:, half : half + 1] for stat in stats]
        peak = fresh[half]
        for level in levels:
            peak = jnp.maximum(peak, level)
        weight = jnp.exp(fresh[half] - peak)
        bottom = weight
        top = weight * value_new
        for owner in range(n_kv):
            weight = jnp.exp(levels[owner] - peak)
            bottom = bottom + weight
            top = top + weight * o_all[owner, half].astype(F32)
        maps.append(top / bottom)
    difference = maps[0] - lam[me // groups] * maps[1]
    normed = (
        difference
        * lax.rsqrt(jnp.mean(difference * difference, axis=1, keepdims=True) + epsilon)
        * head_gain[...]
    )
    h_all[me] = normed.astype(BF16)
    h_copies = exchange("kv", n_kv, lambda peer: h_all.at[me], h_all.at[me], h_s, h_r)
    loads[0].wait()
    wait_recv(h_copies)
    columns = []
    for head in range(n_kv // groups):
        if groups == 1:
            columns.append(h_all[head])
        else:
            columns.append(
                jnp.concatenate(
                    [h_all[head * groups + group].astype(F32) for group in range(groups)], axis=0
                )[:seqs].astype(BF16)
            )
    heads_out = jnp.concatenate(columns, axis=1)
    b_all[me_tp] = jnp.dot(heads_out, wo[...], preferred_element_type=F32).astype(BF16)
    b_copies = exchange("tp", n_tp, lambda peer: b_all.at[me_tp], b_all.at[me_tp], b_s, b_r)
    wait_recv(b_copies)
    branch = b_all[0].astype(F32)
    for index in range(1, n_tp):
        branch = branch + b_all[index].astype(F32)
    residual = (x[...].astype(F32) + branch).astype(BF16)
    res_f = residual.astype(F32)
    sq_all[me] = jnp.broadcast_to(jnp.sum(res_f * res_f, axis=1, keepdims=True), (seqs, 128))
    sq_copies = exchange("kv", n_kv, lambda peer: sq_all.at[me], sq_all.at[me], s_s, s_r)
    normed_mid = (res_f * mid_gain[...]).astype(BF16)
    for index, buf in enumerate((wg, wu)):
        loads[1 + index].wait()
        product = jnp.dot(normed_mid, buf[...], preferred_element_type=F32).astype(FF_LINK)
        product = pad_cols(product, n_kv * chunk)
        for owner in range(n_kv):
            gu_part[owner, index] = product[:, owner * chunk : (owner + 1) * chunk]
    gu_copies = exchange("kv", n_kv, lambda peer: gu_part.at[peer], gu_all.at[me], g_s, g_r)
    gu_all[me] = gu_part[me]
    wait_recv(sq_copies)
    square = sq_all[0]
    for index in range(1, n_kv):
        square = square + sq_all[index]
    scale = lax.rsqrt(square[:, :1] / width + epsilon)
    wait_recv(gu_copies)
    sums = []
    for index in range(2):
        total = gu_all[0, index].astype(F32)
        for owner in range(1, n_kv):
            total = total + gu_all[owner, index].astype(F32)
        sums.append(scale * total)
    hid_all[me] = (sums[0] / (1.0 + jnp.exp(-sums[0])) * sums[1]).astype(BF16)
    i_copies = exchange("kv", n_kv, lambda peer: hid_all.at[me], hid_all.at[me], i_s, i_r)
    loads[3].wait()
    wait_recv(i_copies)
    hidden = jnp.concatenate([hid_all[owner] for owner in range(n_kv)], axis=1)
    hidden = hidden[:, : wd.shape[0]]
    down = jnp.dot(hidden, wd[...], preferred_element_type=F32).astype(BF16)
    own = out.shape[1]
    for index in range(n_tp):
        d_part[index] = down[:, index * own : (index + 1) * own]
    d_copies = exchange("tp", n_tp, lambda peer: d_part.at[peer], d_all.at[me_tp], d_s, d_r)
    d_all[me_tp] = d_part[me_tp]
    base = res_f[:, :own]
    for index in range(1, n_tp):
        base = jnp.where(me_tp == index, res_f[:, index * own : (index + 1) * own], base)
    wait_recv(d_copies)
    mixer = d_all[0].astype(F32)
    for index in range(1, n_tp):
        mixer = mixer + d_all[index].astype(F32)
    out[...] = (base + mixer).astype(BF16)
    wait_send(
        l_copies + o_copies + h_copies + b_copies + sq_copies + gu_copies + i_copies + d_copies
    )


VM = pl.BlockSpec(memory_space=pltpu.VMEM)
ANY = pl.BlockSpec(memory_space=pl.ANY)


def per_device(
    n_kv, n_tp, tokens, attn_gain, w_query, w_key, w_value, cache_keys, cache_values, lambdas,
    head_gain, w_out, mlp_gain, w_gate, w_up, w_down,
):
    seqs, own = tokens.shape
    heads = lambdas.shape[0]
    hd = head_gain.shape[0]
    half = hd // 2
    feats = attn_gain.shape[0]
    width = feats * n_kv
    groups = n_kv // heads
    rows = -(-seqs // groups)
    positions = cache_keys.shape[1]
    units = w_gate.shape[1]
    chunk = 128 * -(-units // (128 * n_kv))
    dma = pltpu.SemaphoreType.DMA
    kv_sems = [dma((n_kv - 1,)), dma((n_kv - 1,))]
    tp_sems = [dma((n_tp - 1,)), dma((n_tp - 1,))]
    sds = jax.ShapeDtypeStruct

    x, q_all, k_own, v_own = pl.pallas_call(
        functools.partial(project_kernel, (n_kv, n_tp, groups, rows, width)),
        out_shape=[
            sds((seqs, feats), BF16), sds((n_kv, rows, hd), BF16),
            sds((rows, hd), BF16), sds((rows, hd), BF16),
        ],
        in_specs=[VM, VM, ANY, ANY, ANY],
        out_specs=[VM] * 4,
        scratch_shapes=[
            pltpu.VMEM((3, feats, heads * hd), BF16),
            pltpu.VMEM((n_tp, seqs, own), BF16),
            pltpu.VMEM((n_kv, seqs, 128), F32),
            pltpu.VMEM((n_kv, 3, rows, hd), QKV_LINK),
            pltpu.VMEM((n_kv, 3, rows, hd), QKV_LINK),
            dma((3,)), *tp_sems, *kv_sems, *kv_sems, *kv_sems,
        ],
        compiler_params=pltpu.CompilerParams(
            collective_id=0, has_side_effects=True, vmem_limit_bytes=24 << 20
        ),
        name="project",
    )(tokens, attn_gain.reshape(1, feats), w_query, w_key, w_value)

    q_heads = q_all.reshape(heads, groups * rows, hd)[:, :seqs]
    q_rows = jnp.transpose(q_heads, (1, 0, 2))
    zero = jnp.zeros_like(q_rows)
    first = lax.broadcasted_iota(jnp.int32, q_rows.shape, 2) < half
    q_blocks = jnp.concatenate(
        [jnp.where(first, q_rows, zero), jnp.where(first, zero, q_rows)], axis=1
    )
    per_step = 2 if seqs % 2 == 0 else 1
    length = positions * heads
    o_maps, l_maps = pl.pallas_call(
        functools.partial(attend_kernel, heads, per_step),
        out_shape=[sds((heads, 2, seqs, hd), BF16), sds((heads, 8, 128), F32)],
        grid=(seqs // per_step,),
        in_specs=[
            pl.BlockSpec((per_step, 2 * heads, hd), lambda i: (i, 0, 0)),
            pl.BlockSpec((per_step, length, hd), lambda i: (i, 0, 0)),
            pl.BlockSpec((per_step, length, hd), lambda i: (i, 0, 0)),
        ],
        out_specs=[
            pl.BlockSpec((heads, 2, seqs, hd), lambda i: (0, 0, 0, 0)),
            pl.BlockSpec((heads, 8, 128), lambda i: (0, 0, 0)),
        ],
        scratch_shapes=[
            pltpu.VMEM((2 * heads, seqs, hd), F32),
            pltpu.VMEM((2 * heads, 128), F32),
        ],
        compiler_params=pltpu.CompilerParams(vmem_limit_bytes=24 << 20),
        name="attend",
    )(
        q_blocks,
        cache_keys.reshape(seqs, length, hd),
        cache_values.reshape(seqs, length, hd),
    )
    if groups > 1:
        extra = groups * rows - seqs
        o_maps = jnp.pad(o_maps, ((0, 0), (0, 0), (0, extra), (0, 0)))
        o_maps = o_maps.reshape(heads, 2, groups, rows, hd).transpose(0, 2, 1, 3, 4)
        o_maps = o_maps.reshape(n_kv, 2, rows, hd)
        l_maps = l_maps[:, :, : groups * rows].reshape(heads, 8, groups, rows)
        l_maps = l_maps.transpose(0, 2, 1, 3).reshape(n_kv, 8, rows)
        l_maps = jnp.pad(l_maps, ((0, 0), (0, 0), (0, 128 - rows)))

    return pl.pallas_call(
        functools.partial(finish_kernel, (n_kv, n_tp, groups, rows, width, chunk)),
        out_shape=sds((seqs, own), BF16),
        in_specs=[pl.BlockSpec(memory_space=pltpu.SMEM)] + [VM] * 8 + [ANY] * 4,
        out_specs=VM,
        scratch_shapes=[
            pltpu.VMEM(w_out.shape, BF16),
            pltpu.VMEM(w_gate.shape, BF16),
            pltpu.VMEM(w_up.shape, BF16),
            pltpu.VMEM(w_down.shape, BF16),
            pltpu.VMEM((n_kv, 2, rows, hd), BF16),
            pltpu.VMEM((n_kv, 8, 128), F32),
            pltpu.VMEM((n_kv, rows, hd), BF16),
            pltpu.VMEM((n_tp, seqs, feats), BF16),
            pltpu.VMEM((n_kv, seqs, 128), F32),
            pltpu.VMEM((n_kv, 2, seqs, chunk), FF_LINK),
            pltpu.VMEM((n_kv, 2, seqs, chunk), FF_LINK),
            pltpu.VMEM((n_kv, seqs, chunk), BF16),
            pltpu.VMEM((n_tp, seqs, own), BF16),
            pltpu.VMEM((n_tp, seqs, own), BF16),
            dma((4,)), *kv_sems, *kv_sems, *kv_sems, *tp_sems,
            *kv_sems, *kv_sems, *kv_sems, *tp_sems,
        ],
        compiler_params=pltpu.CompilerParams(
            collective_id=1, has_side_effects=True, vmem_limit_bytes=30 << 20
        ),
        name="finish",
    )(
        lambdas, o_maps, l_maps, q_all, k_own, v_own, head_gain.reshape(1, hd), x,
        mlp_gain.reshape(1, feats), w_out, w_gate, w_up, w_down,
    )


def solution(mesh):
    in_specs = (
        P(None, ("kv", "tp")), P("kv"), P("kv", "tp"), P("kv", "tp"), P("kv", "tp"),
        P(None, "kv", "tp", None), P(None, "kv", "tp", None), P("tp"), P(),
        P("tp", "kv"), P("kv"), P("kv", "tp"), P("kv", "tp"), P("tp", "kv"),
    )
    return jax.shard_map(
        functools.partial(per_device, mesh.shape["kv"], mesh.shape["tp"]),
        mesh=mesh, in_specs=in_specs, out_specs=P(None, ("kv", "tp")), check_vma=False,
    )
```

time: 442 us -> 97.1 us (0.22)
  blocking collectives: 245 us -> 0 us
  waiting for transfers between devices: 105 us -> 0 us
  Pallas kernels: 0 us -> 69.6 us
  matrix products: 41.8 us -> 0 us
  between operations: 13.3 us -> 0.1 us
  other arithmetic: 11.2 us -> 0.04 us
    all_gather x7 -> x0, blocking collectives: 193 us -> none  [the longest x6 186 us: combined_all(): pieces = jax.tree.map(lambda part: lax.all_gather(part, axis), value)]
    psum x2 -> x0, waiting for transfers between devices: 86.6 us -> none  [the longest x1 52.5 us: per_device(): gate_sum, up_sum = lax.psum((gate_part, up_part), 'kv')]
    pallas_call x0 -> x3, Pallas kernels: none -> 69.6 us  [the longest x1 35 us: per_device(): pl.pallas_call(functools.partial(finish_kernel, (n_kv, n_tp, groups, rows...]
    psum x3 -> x0, blocking collectives: 52.3 us -> none  [the longest x1 22.2 us: per_device(): lax.psum((query_part, key_part, value_part, jnp.sum(gathered_f * gathered...]
    dot_general x11 -> x0, matrix products: 41.8 us -> none  [the longest x2 14.7 us: partial_map(): jnp.einsum('shd,sthd->sht', query_rows[:, :, low:high], cache_keys[:, :,...]
    unnamed x23 -> x29, local copies, waits for them, and re-layouts: 2 us -> 26.7 us
    slice x16 -> x0, local copies, waits for them, and re-layouts: 19.1 us -> none  [the longest x1 17.3 us: partial_map(): cache_keys[:, :, :, low:high]]
    unnamed x4 -> x0, waiting for transfers between devices: 18.8 us -> none
  transfers between devices with their start and end apart: 3 -> 0, of which waited for: 3 -> 0; matrix products, arithmetic and copies ran while one was open for 4% -> 0% of each run, Pallas kernels for 0% -> 0%
where the time goes in v1:
time: 97.1 us; the launch traced here: 96.5 us
  Pallas kernels  69.6 us (72%)
  local copies, waits for them, and re-layouts  26.7 us (27%)
    pallas_call x1, Pallas kernels, per_device(): pl.pallas_call(functools.partial(finish_kernel, (n_kv, n_tp, groups, rows...  35 us
    unnamed x29, local copies, waits for them, and re-layouts  26.7 us
    pallas_call x1, Pallas kernels, per_device(): pl.pallas_call(functools.partial(project_kernel, (n_kv, n_tp, groups, row...  24.3 us
    pallas_call x1, Pallas kernels, per_device(): pl.pallas_call(functools.partial(attend_kernel, heads, per_step), out_sha...  10.3 us

profile of v1, /device:TPU:0, one launch (start us, length us, event | category | flops | bytes accessed | tf_op | source)
XLA Modules:
  0.0 96.5 jit_solution(5808300776704897350)
XLA Ops:
  0.0 0.0 copy-start.4
  0.0 1.2 %copy-done.4 = bf16[512,1024]{1,0:T(8,128)(2,1)S(1)} copy-done((bf16[512,1024]{1,0:T(8,128)(2,1)S(1)}, bf16[512,1024]{1,0:T(8,128)(2,1)}, u32[]{:S(2)}) %copy-start.4) | copy-done | bytes 1048600
  1.2 0.0 copy-start.5
  1.2 1.2 %copy-done.5 = bf16[512,1024]{1,0:T(8,128)(2,1)S(1)} copy-done((bf16[512,1024]{1,0:T(8,128)(2,1)S(1)}, bf16[512,1024]{1,0:T(8,128)(2,1)}, u32[]{:S(2)}) %copy-start.5) | copy-done | bytes 1048600
  2.5 0.0 copy-start.6
  2.5 1.2 %copy-done.6 = bf16[512,1024]{1,0:T(8,128)(2,1)S(1)} copy-done((bf16[512,1024]{1,0:T(8,128)(2,1)S(1)}, bf16[512,1024]{1,0:T(8,128)(2,1)}, u32[]{:S(2)}) %copy-start.6) | copy-done | bytes 1048600
  3.7 0.0 copy-start.8
  3.7 0.7 copy-done.8
  4.4 0.0 copy-start.9
  4.4 0.7 copy-done.9
  5.1 24.3 %project.1 = (bf16[22,512]{1,0:T(8,128)(2,1)S(1)}, bf16[8,22,128]{2,1,0:T(8,128)(2,1)S(1)}, bf16[22,128]{1,0:T(8,128)(2,1)S(1)}, bf16[22,128]{1,0:T(8,128)(2,1)S(1)}) custom-call(bf16[22,128]{1,0:T(8,128)(2,1)S(1)} %copy-done.8, f32[1,512]{1,0:T(1,128)S(1)} %bitcast.11, bf16[512,1024]{1,0:T(8,128)(2,1)S(1)} %copy-done.4, bf16[512,1024]{1,0:T(8,128)(2,1)S(1)} %copy-done.5, ...), custom_call_target="tpu_custom_call" | custom-call | tf_op jit(solution)/shard_map/project/pallas_call | solution.py:328
  29.4 0.0 copy-start
  29.4 4.3 %copy-done = bf16[22,256,8,128]{3,2,1,0:T(8,128)(2,1)S(1)} copy-done((bf16[22,256,8,128]{3,2,1,0:T(8,128)(2,1)S(1)}, bf16[22,256,8,128]{3,2,1,0:T(8,128)(2,1)}, u32[]{:S(2)}) %copy-start) | copy-done | bytes 11534360
  33.7 0.0 copy-start.1
  33.7 4.3 %copy-done.1 = bf16[22,256,8,128]{3,2,1,0:T(8,128)(2,1)S(1)} copy-done((bf16[22,256,8,128]{3,2,1,0:T(8,128)(2,1)S(1)}, bf16[22,256,8,128]{3,2,1,0:T(8,128)(2,1)}, u32[]{:S(2)}) %copy-start.1) | copy-done | bytes 11534360
  38.0 10.3 %attend.1 = (bf16[8,2,22,128]{3,2,1,0:T(8,128)(2,1)S(1)}, f32[8,8,128]{2,1,0:T(8,128)S(1)}) custom-call(bf16[22,16,128]{2,1,0:T(8,128)(2,1)S(1)} %pad_maximum_fusion.q, bf16[22,2048,128]{2,1,0:T(8,128)(2,1)S(1)} %bitcast.9, bf16[22,2048,128]{2,1,0:T(8,128)(2,1)S(1)} %bitcast.10), custom_call_target="tpu_custom_call" | custom-call | tf_op jit(solution)/shard_map/attend/pallas_call | solution.py:359
  48.3 3.1 %copy.17.w_gate = bf16[512,2752]{1,0:T(8,128)(2,1)S(1)} copy(bf16[512,2752]{0,1:T(8,128)(2,1)} %param.25) | data formatting | bytes 5636096 | tf_op args[11]
  51.4 0.0 copy-start.10
  51.4 0.0 copy-start.11
  51.4 0.0 copy-start.12
  51.5 4.6 %copy.18.w_up = bf16[512,2752]{1,0:T(8,128)(2,1)} copy(bf16[512,2752]{0,1:T(8,128)(2,1)} %param.26) | data formatting | bytes 5636096 | tf_op args[12]
  56.0 0.0 copy-done.10
  56.0 0.0 copy-done.11
  56.0 0.0 copy-done.12
  56.0 0.0 copy-start.2
  56.0 1.8 %copy-done.2 = bf16[512,2752]{1,0:T(8,128)(2,1)S(1)} copy-done((bf16[512,2752]{1,0:T(8,128)(2,1)S(1)}, bf16[512,2752]{1,0:T(8,128)(2,1)}, u32[]{:S(2)}) %copy-start.2) | copy-done | bytes 2818072
  57.8 0.0 copy-start.3
  57.8 1.8 %copy-done.3 = bf16[2752,512]{1,0:T(8,128)(2,1)S(1)} copy-done((bf16[2752,512]{1,0:T(8,128)(2,1)S(1)}, bf16[2752,512]{1,0:T(8,128)(2,1)}, u32[]{:S(2)}) %copy-start.3) | copy-done | bytes 2818072
  59.6 0.0 copy-start.7
  59.6 1.2 %copy-done.7 = bf16[1024,512]{1,0:T(8,128)(2,1)S(1)} copy-done((bf16[1024,512]{1,0:T(8,128)(2,1)S(1)}, bf16[1024,512]{1,0:T(8,128)(2,1)}, u32[]{:S(2)}) %copy-start.7) | copy-done | bytes 1048600
  60.9 35.0 %finish.1 = bf16[22,128]{1,0:T(8,128)(2,1)S(1)} custom-call(f32[8]{0:T(128)S(1)} %copy-done.11, bf16[8,2,22,128]{3,2,1,0:T(8,128)(2,1)S(1)} %get-tuple-element.12.o_in, f32[8,8,128]{2,1,0:T(8,128)S(1)} %get-tuple-element.13.l_in, bf16[8,22,128]{2,1,0:T(8,128)(2,1)S(1)} %get-tuple-element.11.q_all, bf16[22,128]{1,0:T(8,128)(2,1)S(1)} %get-tuple-element.14.k_own, ...), custom_call_target="tpu_custom_call" | custom-call | tf_op jit(solution)/shard_map/finish/pallas_call | solution.py:392
  95.9 0.6 copy.22
  (3 shorter events, 0.0 us)
Async XLA Ops:
  0.0 1.2 %copy-start.4 = (bf16[512,1024]{1,0:T(8,128)(2,1)S(1)}, bf16[512,1024]{1,0:T(8,128)(2,1)}, u32[]{:S(2)}) copy-start(bf16[512,1024]{1,0:T(8,128)(2,1)} %wq.1) | copy-start | bytes 3145732
  1.2 1.2 %copy-start.5 = (bf16[512,1024]{1,0:T(8,128)(2,1)S(1)}, bf16[512,1024]{1,0:T(8,128)(2,1)}, u32[]{:S(2)}) copy-start(bf16[512,1024]{1,0:T(8,128)(2,1)} %wk.1) | copy-start | bytes 3145732
  2.5 1.2 %copy-start.6 = (bf16[512,1024]{1,0:T(8,128)(2,1)S(1)}, bf16[512,1024]{1,0:T(8,128)(2,1)}, u32[]{:S(2)}) copy-start(bf16[512,1024]{1,0:T(8,128)(2,1)} %wv.1) | copy-start | bytes 3145732
  3.7 0.7 copy-start.8
  4.4 0.7 copy-start.9
  29.4 4.3 %copy-start = (bf16[22,256,8,128]{3,2,1,0:T(8,128)(2,1)S(1)}, bf16[22,256,8,128]{3,2,1,0:T(8,128)(2,1)}, u32[]{:S(2)}) copy-start(bf16[22,256,8,128]{3,2,1,0:T(8,128)(2,1)} %param.19) | copy-start | bytes 34603012
  33.7 4.3 %copy-start.1 = (bf16[22,256,8,128]{3,2,1,0:T(8,128)(2,1)S(1)}, bf16[22,256,8,128]{3,2,1,0:T(8,128)(2,1)}, u32[]{:S(2)}) copy-start(bf16[22,256,8,128]{3,2,1,0:T(8,128)(2,1)} %param.20) | copy-start | bytes 34603012
  51.4 4.6 %copy-start.10 = (f32[512]{0:T(512)S(1)}, f32[512]{0:T(512)}, u32[]{:S(2)}) copy-start(f32[512]{0:T(512)} %param.24) | copy-start | bytes 6148
  51.4 4.6 %copy-start.11 = (f32[8]{0:T(128)S(1)}, f32[8]{0:T(128)}, u32[]{:S(2)}) copy-start(f32[8]{0:T(128)} %lam.1) | copy-start | bytes 100
  51.4 4.6 %copy-start.12 = (f32[128]{0:T(128)S(1)}, f32[128]{0:T(128)}, u32[]{:S(2)}) copy-start(f32[128]{0:T(128)} %param.22) | copy-start | bytes 1540
  56.0 1.8 %copy-start.2 = (bf16[512,2752]{1,0:T(8,128)(2,1)S(1)}, bf16[512,2752]{1,0:T(8,128)(2,1)}, u32[]{:S(2)}) copy-start(bf16[512,2752]{1,0:T(8,128)(2,1)} %copy.18.w_up) | copy-start | bytes 8454148
  57.8 1.8 %copy-start.3 = (bf16[2752,512]{1,0:T(8,128)(2,1)S(1)}, bf16[2752,512]{1,0:T(8,128)(2,1)}, u32[]{:S(2)}) copy-start(bf16[2752,512]{1,0:T(8,128)(2,1)} %w_down.1) | copy-start | bytes 8454148
  59.6 1.2 %copy-start.7 = (bf16[1024,512]{1,0:T(8,128)(2,1)S(1)}, bf16[1024,512]{1,0:T(8,128)(2,1)}, u32[]{:S(2)}) copy-start(bf16[1024,512]{1,0:T(8,128)(2,1)} %w_out.1) | copy-start | bytes 3145732

commit v2 on v1

v2 whole, which is shorter than its diff:
```python
import functools

import jax
import jax.numpy as jnp
from jax import lax
from jax.experimental import pallas as pl
from jax.experimental.pallas import tpu as pltpu
from jax.sharding import PartitionSpec as P

epsilon = 1e-06
MESH = pl.DeviceIdType.MESH
F32 = jnp.float32
BF16 = jnp.bfloat16
Q_LINK = jnp.bfloat16
KV_LINK = jnp.float32
FF_LINK = jnp.bfloat16


def peers(axis, count):
    me = lax.axis_index(axis)
    return [(step, lax.rem(me + step, count)) for step in range(1, count)]


def greet(n_kv, n_tp):
    barrier = pltpu.get_barrier_semaphore()
    for axis, count in (("kv", n_kv), ("tp", n_tp)):
        for _, peer in peers(axis, count):
            pl.semaphore_signal(barrier, inc=1, device_id={axis: peer}, device_id_type=MESH)
    pl.semaphore_wait(barrier, n_kv + n_tp - 2)


def exchange(axis, count, source, target, send_sem, recv_sem):
    copies = []
    for step, peer in peers(axis, count):
        copy = pltpu.make_async_remote_copy(
            src_ref=source(peer),
            dst_ref=target,
            send_sem=send_sem.at[step - 1],
            recv_sem=recv_sem.at[step - 1],
            device_id={axis: peer},
            device_id_type=MESH,
        )
        copy.start()
        copies.append(copy)
    return copies


def wait_recv(copies):
    for copy in copies:
        copy.wait_recv()


def wait_send(copies):
    for copy in copies:
        copy.wait_send()


def pad_rows(value, rows):
    if value.shape[0] == rows:
        return value
    return jnp.concatenate(
        [value, jnp.zeros((rows - value.shape[0],) + value.shape[1:], value.dtype)], axis=0
    )


def pad_cols(value, cols):
    if value.shape[1] == cols:
        return value
    return jnp.concatenate(
        [value, jnp.zeros((value.shape[0], cols - value.shape[1]), value.dtype)], axis=1
    )


def layer_kernel(
    dims, tok_in, gain_in, wq_in, wk_in, wv_in, keys_in, values_in, lam_in, head_gain_in, w_out_in,
    mid_gain_in, w_gate_in, w_up_in, w_down_in,
    out,
    tok, gain, lam, head_gain, mid_gain, wq, wk, wv, keys, values, wo, wg, wu, wd,
    tok_all, sq_all, q_part, q_got, kv_part, kv_got, q_all, q_seq, acc, lse,
    o_in, o_all, l_in, l_all, h_all, b_all, mid_all, gu_part, gu_all, hid_all, d_part, d_all,
    w_sem, k_sem, v_sem, *sems,
):
    n_kv, n_tp, groups, rows, width, chunk, per_step = dims
    seqs, own = out.shape
    heads = n_kv // groups
    hd = head_gain.shape[1]
    half_dim = hd // 2
    score_scale = half_dim ** (-0.5)
    length = keys.shape[1]
    steps = seqs // per_step
    pairs = [(sems[2 * at], sems[2 * at + 1]) for at in range(len(sems) // 2)]
    t_sem, sq_sem, q_sem, qa_sem, kv_sem, l_sem, o_sem, h_sem, b_sem, m_sem = pairs[:10]
    g_sems, i_sem, d_sem = pairs[10:12], pairs[12], pairs[13]

    def load(index, source, target):
        copy = pltpu.make_async_copy(source, target, w_sem.at[index])
        copy.start()
        return copy

    load_tok = load(0, tok_in, tok)
    load_gain = load(1, gain_in, gain)
    load_q = load(2, wq_in, wq)
    load_k = load(3, wk_in, wk)
    load_v = load(4, wv_in, wv)

    def cache_copies(step):
        at = pl.ds(step * per_step, per_step)
        return (
            pltpu.make_async_copy(keys_in.at[at], keys.at[at], k_sem.at[step]),
            pltpu.make_async_copy(values_in.at[at], values.at[at], v_sem.at[step]),
        )

    for step in range(steps):
        for copy in cache_copies(step):
            copy.start()
    load_lam = load(5, lam_in, lam)
    load_hg = load(6, head_gain_in, head_gain)
    load_mg = load(7, mid_gain_in, mid_gain)
    load_wo = load(8, w_out_in, wo)
    load_wg = load(9, w_gate_in, wg)
    load_wu = load(10, w_up_in, wu)
    units = w_down_in.shape[0]
    load_wd = load(11, w_down_in, wd.at[pl.ds(0, units)])
    if units < n_kv * chunk:
        wd[units:, :] = jnp.zeros((n_kv * chunk - units, wd.shape[1]), BF16)

    greet(n_kv, n_tp)
    me = lax.axis_index("kv")
    me_tp = lax.axis_index("tp")
    load_tok.wait()
    tok_copies = exchange("tp", n_tp, lambda peer: tok, tok_all.at[me_tp], *t_sem)
    tok_all[me_tp] = tok[...]
    load_gain.wait()
    wait_recv(tok_copies)
    xf = jnp.concatenate([tok_all[index] for index in range(n_tp)], axis=1).astype(F32)
    normed = (xf * gain[...]).astype(BF16)

    def project(buf, part, index, link):
        product = jnp.dot(normed, buf[...], preferred_element_type=F32).astype(link)
        product = pad_rows(product, groups * rows)
        for owner in range(n_kv):
            head, group = owner // groups, owner % groups
            part[owner, index] = product[
                group * rows : (group + 1) * rows, head * hd : (head + 1) * hd
            ]

    def gathered_sum(got, index):
        total = got[0, index].astype(F32)
        for owner in range(1, n_kv):
            total = total + got[owner, index].astype(F32)
        return total

    load_q.wait()
    project(wq, q_part, 0, Q_LINK)
    q_copies = exchange("kv", n_kv, lambda peer: q_part.at[peer], q_got.at[me], *q_sem)
    q_got[me] = q_part[me]
    sq_all[me] = jnp.broadcast_to(jnp.sum(xf * xf, axis=1, keepdims=True), (seqs, 128))
    sq_copies = exchange("kv", n_kv, lambda peer: sq_all.at[me], sq_all.at[me], *sq_sem)
    load_k.wait()
    project(wk, kv_part, 0, KV_LINK)
    load_v.wait()
    project(wv, kv_part, 1, KV_LINK)
    kv_got[me] = kv_part[me]
    wait_recv(q_copies)
    total = gathered_sum(q_got, 0)
    wait_recv(sq_copies)
    square = sq_all[0]
    for index in range(1, n_kv):
        square = square + sq_all[index]
    scale = lax.rsqrt(square[:, :1] / width + epsilon)
    if groups > 1:
        scale = pad_rows(scale, groups * rows)
        group_of = lax.rem(me, groups)
        mine = scale[:rows]
        for group in range(1, groups):
            mine = jnp.where(group_of == group, scale[group * rows : (group + 1) * rows], mine)
        scale = mine
    q_own = (scale * total).astype(BF16)
    q_all[me] = q_own
    qa_copies = exchange("kv", n_kv, lambda peer: q_all.at[me], q_all.at[me], *qa_sem)
    kv_copies = exchange("kv", n_kv, lambda peer: kv_part.at[peer], kv_got.at[me], *kv_sem)
    wait_recv(qa_copies)
    for owner in range(n_kv):
        head, group = owner // groups, owner % groups
        q_seq[group * rows : (group + 1) * rows, head : head + 1, :] = q_all[owner].astype(F32)[
            :, None, :
        ]

    row = lax.broadcasted_iota(jnp.int32, (2 * heads * per_step, length), 0)
    col = lax.broadcasted_iota(jnp.int32, (2 * heads * per_step, length), 1)
    keep = lax.rem(col, heads) == lax.rem(row, heads)
    stat_lane = lax.broadcasted_iota(jnp.int32, (2 * heads, 128), 1)
    q_lane = lax.broadcasted_iota(jnp.int32, (heads, hd), 1)
    lse[...] = jnp.zeros_like(lse)
    l_in[...] = jnp.zeros_like(l_in)

    def queries(seq):
        vec = q_seq[seq]
        return jnp.concatenate(
            [jnp.where(q_lane < half_dim, vec, 0.0), jnp.where(q_lane < half_dim, 0.0, vec)],
            axis=0,
        ).astype(BF16)

    def wide(parts):
        return parts[0] if per_step == 1 else jnp.concatenate(parts, axis=1)

    def attend(at):
        span = range(at * per_step, (at + 1) * per_step)
        blank = jnp.zeros((2 * heads, hd), BF16)
        query = jnp.concatenate(
            [wide([queries(seq) if other == seq else blank for other in span]) for seq in span],
            axis=0,
        )
        scores = lax.dot_general(
            query, wide([keys[seq] for seq in span]), (((1,), (1,)), ((), ())),
            preferred_element_type=F32,
        )
        scores = jnp.where(keep, scores * score_scale, -jnp.inf)
        peak = jnp.max(scores, axis=1, keepdims=True)
        weights = jnp.exp(scores - peak)
        total = jnp.sum(weights, axis=1, keepdims=True)
        summed = jnp.dot(
            weights.astype(BF16), wide([values[seq] for seq in span]), preferred_element_type=F32
        )
        result = summed / total
        level = peak + jnp.log(total)
        stats = lse[...]
        for index, seq in enumerate(span):
            part = slice(index * 2 * heads, (index + 1) * 2 * heads)
            acc[:, seq : seq + 1, :] = result[part, index * hd : (index + 1) * hd][:, None, :]
            stats = jnp.where(stat_lane == seq, level[part], stats)
        lse[...] = stats

    for step in range(steps):
        for copy in cache_copies(step):
            copy.wait()
    for step in range(steps):
        attend(step)

    for owner in range(n_kv):
        head, group = owner // groups, owner % groups
        span = slice(group * rows, (group + 1) * rows)
        for half in range(2):
            at = half * heads + head
            l_in[owner, half : half + 1, :] = pad_cols(lse[at : at + 1, span], 128)
    l_copies = exchange("kv", n_kv, lambda peer: l_in.at[peer], l_all.at[me], *l_sem)
    for owner in range(n_kv):
        head, group = owner // groups, owner % groups
        span = slice(group * rows, (group + 1) * rows)
        for half in range(2):
            o_in[owner, half] = acc[half * heads + head, span, :].astype(BF16)
    o_copies = exchange("kv", n_kv, lambda peer: o_in.at[peer], o_all.at[me], *o_sem)
    l_all[me] = l_in[me]
    o_all[me] = o_in[me]
    wait_recv(kv_copies)
    k_own = (scale * gathered_sum(kv_got, 0)).astype(BF16).astype(F32)
    value_new = (scale * gathered_sum(kv_got, 1)).astype(BF16).astype(F32)
    product = q_own.astype(F32) * k_own
    lane = lax.broadcasted_iota(jnp.int32, product.shape, 1)
    low = jnp.where(lane < half_dim, product, 0.0)
    high = jnp.where(lane < half_dim, 0.0, product)
    fresh = [jnp.sum(part, axis=1, keepdims=True) * score_scale for part in (low, high)]
    load_lam.wait()
    load_hg.wait()
    load_mg.wait()
    at_head = lax.broadcasted_iota(jnp.int32, lam.shape, 1) == me // groups
    lam_own = jnp.sum(jnp.where(at_head, lam[...], 0.0), axis=1, keepdims=True)
    wait_recv(l_copies)
    stats = []
    for start in range(0, n_kv, 16):
        owners = range(start, min(start + 16, n_kv))
        stacked = pad_rows(jnp.concatenate([l_all[owner] for owner in owners], axis=0), 128)
        turned = jnp.transpose(stacked)
        stats += [turned[:rows, 8 * at : 8 * at + 2] for at in range(len(owners))]
    wait_recv(o_copies)
    maps = []
    for half in range(2):
        levels = [stat[:, half : half + 1] for stat in stats]
        peak = fresh[half]
        for level in levels:
            peak = jnp.maximum(peak, level)
        weight = jnp.exp(fresh[half] - peak)
        bottom = weight
        top = weight * value_new
        for owner in range(n_kv):
            weight = jnp.exp(levels[owner] - peak)
            bottom = bottom + weight
            top = top + weight * o_all[owner, half].astype(F32)
        maps.append(top / bottom)
    difference = maps[0] - lam_own * maps[1]
    normed = (
        difference
        * lax.rsqrt(jnp.mean(difference * difference, axis=1, keepdims=True) + epsilon)
        * head_gain[...]
    )
    h_all[me] = normed.astype(BF16)
    h_copies = exchange("kv", n_kv, lambda peer: h_all.at[me], h_all.at[me], *h_sem)
    load_wo.wait()
    wait_recv(h_copies)
    columns = []
    for head in range(n_kv // groups):
        if groups == 1:
            columns.append(h_all[head])
        else:
            columns.append(
                jnp.concatenate(
                    [h_all[head * groups + group].astype(F32) for group in range(groups)], axis=0
                )[:seqs].astype(BF16)
            )
    heads_out = jnp.concatenate(columns, axis=1)
    b_all[me_tp] = jnp.dot(heads_out, wo[...], preferred_element_type=F32).astype(BF16)
    b_copies = exchange("tp", n_tp, lambda peer: b_all.at[me_tp], b_all.at[me_tp], *b_sem)
    wait_recv(b_copies)
    branch = b_all[0].astype(F32)
    for index in range(1, n_tp):
        branch = branch + b_all[index].astype(F32)
    residual = (xf + branch).astype(BF16)
    res_f = residual.astype(F32)
    mid_all[me] = jnp.broadcast_to(jnp.sum(res_f * res_f, axis=1, keepdims=True), (seqs, 128))
    mid_copies = exchange("kv", n_kv, lambda peer: mid_all.at[me], mid_all.at[me], *m_sem)
    normed_mid = (res_f * mid_gain[...]).astype(BF16)
    gu_copies = []
    for index, (ready, buf) in enumerate(((load_wg, wg), (load_wu, wu))):
        ready.wait()
        product = lax.dot_general(
            normed_mid, buf[...], (((1,), (1,)), ((), ())), preferred_element_type=F32
        ).astype(FF_LINK)
        product = pad_cols(product, n_kv * chunk)
        for owner in range(n_kv):
            gu_part[index, owner] = product[:, owner * chunk : (owner + 1) * chunk]
        gu_copies += exchange(
            "kv", n_kv, lambda peer: gu_part.at[index, peer], gu_all.at[index, me], *g_sems[index]
        )
        gu_all[index, me] = gu_part[index, me]
    wait_recv(mid_copies)
    square = mid_all[0]
    for index in range(1, n_kv):
        square = square + mid_all[index]
    scale = lax.rsqrt(square[:, :1] / width + epsilon)
    wait_recv(gu_copies)
    sums = []
    for index in range(2):
        total = gu_all[index, 0].astype(F32)
        for owner in range(1, n_kv):
            total = total + gu_all[index, owner].astype(F32)
        sums.append(scale * total)
    hid_all[me] = (sums[0] / (1.0 + jnp.exp(-sums[0])) * sums[1]).astype(BF16)
    i_copies = exchange("kv", n_kv, lambda peer: hid_all.at[me], hid_all.at[me], *i_sem)
    load_wd.wait()
    down = None
    for step in range(n_kv):
        if step > 0:
            i_copies[step - 1].wait_recv()
        owner = lax.rem(me + n_kv - step, n_kv)
        share = jnp.dot(
            hid_all[owner],
            wd[pl.ds(pl.multiple_of(owner * chunk, chunk), chunk), :],
            preferred_element_type=F32,
        )
        down = share if down is None else down + share
    down = down.astype(BF16)
    own = out.shape[1]
    for index in range(n_tp):
        d_part[index] = down[:, index * own : (index + 1) * own]
    d_copies = exchange("tp", n_tp, lambda peer: d_part.at[peer], d_all.at[me_tp], *d_sem)
    d_all[me_tp] = d_part[me_tp]
    base = res_f[:, :own]
    for index in range(1, n_tp):
        base = jnp.where(me_tp == index, res_f[:, index * own : (index + 1) * own], base)
    wait_recv(d_copies)
    mixer = d_all[0].astype(F32)
    for index in range(1, n_tp):
        mixer = mixer + d_all[index].astype(F32)
    out[...] = (base + mixer).astype(BF16)
    wait_send(
        tok_copies + q_copies + sq_copies + qa_copies + kv_copies + l_copies + o_copies
        + h_copies + b_copies + mid_copies + gu_copies + i_copies + d_copies
    )


ANY = pl.BlockSpec(memory_space=pl.ANY)


def per_device(
    n_kv, n_tp, tokens, attn_gain, w_query, w_key, w_value, cache_keys, cache_values, lambdas,
    head_gain, w_out, mlp_gain, w_gate, w_up, w_down,
):
    seqs, own = tokens.shape
    heads = lambdas.shape[0]
    hd = head_gain.shape[0]
    feats = attn_gain.shape[0]
    width = feats * n_kv
    groups = n_kv // heads
    rows = -(-seqs // groups)
    units = w_gate.shape[1]
    chunk = 128 * -(-units // (128 * n_kv))
    length = cache_keys.shape[1] * heads
    per_step = 2 if seqs % 2 == 0 else 1
    dma = pltpu.SemaphoreType.DMA
    kv_sems = [dma((n_kv - 1,)), dma((n_kv - 1,))]
    tp_sems = [dma((n_tp - 1,)), dma((n_tp - 1,))]
    vm = pltpu.VMEM
    return pl.pallas_call(
        functools.partial(layer_kernel, (n_kv, n_tp, groups, rows, width, chunk, per_step)),
        out_shape=jax.ShapeDtypeStruct((seqs, own), BF16),
        in_specs=[ANY] * 14,
        out_specs=pl.BlockSpec(memory_space=pltpu.VMEM),
        scratch_shapes=[
            vm((seqs, own), BF16),
            vm((1, feats), F32),
            vm((1, heads), F32),
            vm((1, hd), F32),
            vm((1, feats), F32),
            vm(w_query.shape, BF16),
            vm(w_key.shape, BF16),
            vm(w_value.shape, BF16),
            vm((seqs, length, hd), BF16),
            vm((seqs, length, hd), BF16),
            vm(w_out.shape, BF16),
            vm((units, feats), BF16),
            vm((units, feats), BF16),
            vm((n_kv * chunk, w_down.shape[1]), BF16),
            vm((n_tp, seqs, own), BF16),
            vm((n_kv, seqs, 128), F32),
            vm((n_kv, 1, rows, hd), Q_LINK),
            vm((n_kv, 1, rows, hd), Q_LINK),
            vm((n_kv, 2, rows, hd), KV_LINK),
            vm((n_kv, 2, rows, hd), KV_LINK),
            vm((n_kv, rows, hd), BF16),
            vm((groups * rows, heads, hd), F32),
            vm((2 * heads, groups * rows, hd), F32),
            vm((2 * heads, 128), F32),
            vm((n_kv, 2, rows, hd), BF16),
            vm((n_kv, 2, rows, hd), BF16),
            vm((n_kv, 8, 128), F32),
            vm((n_kv, 8, 128), F32),
            vm((n_kv, rows, hd), BF16),
            vm((n_tp, seqs, feats), BF16),
            vm((n_kv, seqs, 128), F32),
            vm((2, n_kv, seqs, chunk), FF_LINK),
            vm((2, n_kv, seqs, chunk), FF_LINK),
            vm((n_kv, seqs, chunk), BF16),
            vm((n_tp, seqs, own), BF16),
            vm((n_tp, seqs, own), BF16),
            dma((12,)), dma((seqs // per_step,)), dma((seqs // per_step,)),
            *tp_sems, *(kv_sems * 7), *tp_sems, *(kv_sems * 4), *tp_sems,
        ],
        compiler_params=pltpu.CompilerParams(
            collective_id=0, has_side_effects=True, vmem_limit_bytes=62 << 20
        ),
        name="layer",
    )(
        tokens, attn_gain.reshape(1, feats), w_query, w_key, w_value,
        cache_keys.reshape(seqs, length, hd), cache_values.reshape(seqs, length, hd),
        lambdas.reshape(1, heads), head_gain.reshape(1, hd), w_out, mlp_gain.reshape(1, feats),
        w_gate.T, w_up.T, w_down,
    )


def solution(mesh):
    in_specs = (
        P(None, ("kv", "tp")), P("kv"), P("kv", "tp"), P("kv", "tp"), P("kv", "tp"),
        P(None, "kv", "tp", None), P(None, "kv", "tp", None), P("tp"), P(),
        P("tp", "kv"), P("kv"), P("kv", "tp"), P("kv", "tp"), P("tp", "kv"),
    )
    return jax.shard_map(
        functools.partial(per_device, mesh.shape["kv"], mesh.shape["tp"]),
        mesh=mesh, in_specs=in_specs, out_specs=P(None, ("kv", "tp")), check_vma=False,
    )
```

time: 97.1 us -> 61.5 us (0.63)
  local copies, waits for them, and re-layouts: 26.7 us -> 1.29 us
  Pallas kernels: 69.6 us -> 60 us
    unnamed x29 -> x1, local copies, waits for them, and re-layouts: 26.7 us -> 1.29 us
    pallas_call x3 -> x1, Pallas kernels: 69.6 us -> 60 us  [per_device(): pl.pallas_call(functools.partial(layer_kernel, (n_kv, n_tp, groups, rows,...]
where the time goes in v2:
time: 61.5 us; the launch traced here: 61.3 us
  Pallas kernels  60 us (98%)
  local copies, waits for them, and re-layouts  1.29 us (2%)
    pallas_call x1, Pallas kernels, per_device(): pl.pallas_call(functools.partial(layer_kernel, (n_kv, n_tp, groups, rows,...  60 us
    unnamed x1, local copies, waits for them, and re-layouts  1.29 us

profile of v2, /device:TPU:0, one launch (start us, length us, event | category | flops | bytes accessed | tf_op | source)
XLA Modules:
  0.0 61.3 jit_solution(4907523235028746643)
XLA Ops:
  0.0 60.0 %layer.1 = bf16[22,128]{1,0:T(8,128)(2,1)} custom-call(bf16[22,128]{1,0:T(8,128)(2,1)} %tok_in.1, f32[1,512]{1,0:T(1,128)} %bitcast.12, bf16[512,1024]{1,0:T(8,128)(2,1)} %wq_in.1, bf16[512,1024]{1,0:T(8,128)(2,1)} %wk_in.1, bf16[512,1024]{1,0:T(8,128)(2,1)} %wv_in.1, bf16[22,2048,128]{2,1,0:T(8,128)(2,1)} %bitcast.8, bf16[22,2048,128]{2,1,0:T(8,128)(2,1)} %bitcast.9, ...), custom_call_target="tpu_custom_call" | custom-call | tf_op jit(solution)/shard_map/layer/pallas_call | solution.py:403
  60.0 1.3 %copy.16 = bf16[22,128]{1,0:T(8,128)(2,1)} copy(bf16[22,128]{1,0:T(8,128)(2,1)} %layer.1) | data formatting | bytes 11264
